TPU v7x, 32 devices: a whole 2x2x4 slice. The times are simulated.
32 devices in a mesh: ra: 8 (over z, x), cb: 4 (over y, core).
Axes of the slice: x: 2, y: 2, z: 4, core: 2. Of those that a mesh axis runs over, the one named last changes fastest.
Arguments:
- tokens: bfloat16 [384, 4096], P(None, 'ra'), may hold values from -260 to 260
- up_weight: float32 [2, 4096, 16384], P(None, 'ra', 'cb'), may hold values from -0.125 to 0.125
- up_scale: float32 [2, 16384], P(None, 'cb'), may hold values from 0.5 to 2
- down_weight: float32 [2, 16384, 4096], P(None, 'cb', 'ra'), may hold values from -0.046875 to 0.046875
- down_scale: float32 [2, 4096], P(None, 'ra'), may hold values from 0.7 to 14
- pre_gain: float32 [2, 4096], P(None, 'ra'), may hold values from 0.1 to 1.9
- post_gain: float32 [2, 4096], P(None, 'ra'), may hold values from 0.1 to 1.9
Outputs:
- stream_out: bfloat16 [384, 4096], P(None, 'ra')
All inputs are finite; a program needn't handle non-finite values.
Results may differ from a plain program's by a relative error of at most 0.023.
Values may be sent and summed in bfloat16 or wider, within the bound.
A program may use at most 128 MiB of HBM per device.

v0:
```python
import jax
import jax.numpy as jnp
from jax import lax
from jax.sharding import PartitionSpec as P

norm_eps = 1e-06
residual_keep = 0.5


def local(tokens, up_weight, up_scale, down_weight, down_scale, pre_gain, post_gain):
    values = tokens.astype(jnp.float32)
    model_width = tokens.shape[1] * lax.axis_size("ra")
    stream = tokens
    for sublayer in range(up_weight.shape[0]):
        scaled = (values * pre_gain[sublayer][None, :]).astype(jnp.bfloat16)
        up_matrix = up_weight[sublayer].astype(jnp.bfloat16)
        down_matrix = down_weight[sublayer].astype(jnp.bfloat16)
        partial_up = jnp.dot(scaled, up_matrix, preferred_element_type=jnp.float32)
        whole_up = lax.psum(partial_up.astype(jnp.bfloat16), "ra").astype(jnp.float32)
        hidden = jnp.square(jax.nn.relu(whole_up * up_scale[sublayer][None, :])).astype(
            jnp.bfloat16
        )
        partial_down = jnp.dot(hidden, down_matrix, preferred_element_type=jnp.float32)
        summed = lax.psum(partial_down.astype(jnp.bfloat16), "cb").astype(jnp.float32)
        branch_in = summed * down_scale[sublayer][None, :]
        post_squares = lax.psum(jnp.sum(branch_in * branch_in, axis=1), "ra")
        inv_post = lax.rsqrt(post_squares / model_width + norm_eps)[:, None]
        branch = branch_in * inv_post * post_gain[sublayer][None, :]
        stream = (residual_keep * values + branch).astype(jnp.bfloat16)
        values = stream.astype(jnp.float32)
    return stream


def solution(mesh):
    return jax.shard_map(
        local,
        mesh=mesh,
        in_specs=(
            P(None, "ra"),
            P(None, "ra", "cb"),
            P(None, "cb"),
            P(None, "cb", "ra"),
            P(None, "ra"),
            P(None, "ra"),
            P(None, "ra"),
        ),
        out_specs=P(None, "ra"),
        check_vma=False,
    )
```

profile of v0, /device:TPU:0, one launch (start us, length us, event | category | flops | bytes accessed | tf_op | source)
XLA Modules:
  0.0 411.9 jit_solution(7826004567021123031)
XLA Ops:
  6.5 6.5 %convert.8 = bf16[2,512,4096]{2,1,0:T(8,128)(2,1)S(1)} convert(f32[2,512,4096]{2,1,0:T(8,128)} %param.8) | non-fusion elementwise | flops 4194304 | bytes 25165824 | tf_op jit(solution)/shard_map/convert.3
  13.1 3.2 copy-done
  16.3 3.5 convolution_convert_fusion.1
  19.8 0.0 all-reduce.5.cloned.1.call-update
  19.8 0.0 copy-start.5
  19.9 0.0 all-reduce.7.cloned.1.call-start
  19.9 9.0 %convert.9 = bf16[2,4096,512]{2,1,0:T(8,128)(2,1)} convert(f32[2,4096,512]{2,1,0:T(8,128)} %param.10) | non-fusion elementwise | flops 4194304 | bytes 25165824 | tf_op jit(solution)/shard_map/convert.2
  29.0 122.7 %all-reduce.5.cloned.1.call-done = bf16[384,4096]{1,0:T(8,128)(2,1)} async-done(((bf16[384,4096]{1,0:T(8,128)(2,1)}), bf16[384,4096]{1,0:T(8,128)(2,1)}) %all-reduce.5.cloned.1.call-update) | async-done | bytes 3145744 | tf_op jit(solution)/shard_map/psum | solution.py:19
  151.6 5.7 %fusion.6 = bf16[384,512]{1,0:T(8,128)(2,1)} fusion(bf16[2,4096,512]{2,1,0:T(8,128)(2,1)} %convert.9, bf16[384,4096]{1,0:T(8,128)(2,1)} %all-reduce.5.cloned.1.call-done, f32[4096]{0:T(1024)S(1)} %bitcast.30), kind=kOutput, calls=%fused_computation.14 | convolution fusion | flops 1618673664 | bytes 7749632 | tf_op jit(solution)/shard_map/dot_general | solution.py:23
  157.4 0.0 all-reduce.7.cloned.1.call-update
  157.4 0.0 all-reduce.9.cloned.1.call-start
  157.4 31.9 %all-reduce.7.cloned.1.call-done = bf16[384,512]{1,0:T(8,128)(2,1)} async-done(((bf16[384,512]{1,0:T(8,128)(2,1)}), bf16[384,512]{1,0:T(8,128)(2,1)}) %all-reduce.7.cloned.1.call-update) | async-done | bytes 393232 | tf_op jit(solution)/shard_map/psum | solution.py:24
  189.4 1.2 multiply_reduce_fusion.1
  190.5 21.3 %psum.44 = f32[384]{0:T(512)S(1)} all-reduce(f32[384]{0:T(512)S(1)} %multiply_reduce_fusion.1), channel_id=1, replica_groups=mesh['ra'=8,'cb'=4] {'ra'}, use_global_device_ids=true, to_apply=%region_3.4 | all-reduce | flops 384 | bytes 3072 | tf_op jit(solution)/shard_map/psum | solution.py:26
  211.9 5.9 %convolution_convert_fusion = bf16[384,4096]{1,0:T(8,128)(2,1)} fusion(bf16[2,512,4096]{2,1,0:T(8,128)(2,1)} %copy-done, f32[512]{0:T(512)S(1)} %bitcast.34, bf16[384,512]{1,0:T(8,128)(2,1)S(1)} %copy-done.2, bf16[384,512]{1,0:T(8,128)(2,1)} %all-reduce.7.cloned.1.call-done, f32[512]{0:T(512)S(1)} %bitcast.32, f32[384]{0:T(512)S(1)} %add_rsqrt_fusion.1, ...), kind=kOutput, calls=%fused_computation.2 | convolution fusion | flops 1614348288 | bytes 8134144 | tf_op jit(solution)/shard_map/dot_general | solution.py:18
  217.8 0.0 all-reduce.9.cloned.1.call-update
  217.8 0.0 all-reduce.11.cloned.1.call-start
  217.8 125.1 %all-reduce.9.cloned.1.call-done = bf16[384,4096]{1,0:T(8,128)(2,1)} async-done(((bf16[384,4096]{1,0:T(8,128)(2,1)}), bf16[384,4096]{1,0:T(8,128)(2,1)}) %all-reduce.9.cloned.1.call-update) | async-done | bytes 3145744 | tf_op jit(solution)/shard_map/psum | solution.py:19
  342.9 5.7 %fusion.7 = bf16[384,512]{1,0:T(8,128)(2,1)} fusion(bf16[2,4096,512]{2,1,0:T(8,128)(2,1)} %convert.9, bf16[384,4096]{1,0:T(8,128)(2,1)} %all-reduce.9.cloned.1.call-done, f32[4096]{0:T(1024)S(1)} %bitcast.29), kind=kOutput, calls=%fused_computation.15 | convolution fusion | flops 1618673664 | bytes 7749632 | tf_op jit(solution)/shard_map/dot_general | solution.py:23
  348.7 0.0 all-reduce.11.cloned.1.call-update
  348.7 32.0 %all-reduce.11.cloned.1.call-done = bf16[384,512]{1,0:T(8,128)(2,1)} async-done(((bf16[384,512]{1,0:T(8,128)(2,1)}), bf16[384,512]{1,0:T(8,128)(2,1)}) %all-reduce.11.cloned.1.call-update) | async-done | bytes 393232 | tf_op jit(solution)/shard_map/psum | solution.py:24
  380.7 1.2 multiply_reduce_fusion
  381.9 21.3 %psum.47 = f32[384]{0:T(512)S(1)} all-reduce(f32[384]{0:T(512)S(1)} %multiply_reduce_fusion), channel_id=1, replica_groups=mesh['ra'=8,'cb'=4] {'ra'}, use_global_device_ids=true, to_apply=%region_7.8 | all-reduce | flops 384 | bytes 3072 | tf_op jit(solution)/shard_map/psum | solution.py:26
  403.2 2.1 fusion.12
  (19 shorter events, 0.1 us)
Async XLA Ops:
  6.5 6.5 %copy-start.4 = (f32[2,512]{1,0:T(2,128)S(1)}, f32[2,512]{1,0:T(2,128)}, u32[]{:S(2)}) copy-start(f32[2,512]{1,0:T(2,128)} %param.12) | copy-start | bytes 12292
  6.5 9.8 %copy-start.2 = (bf16[384,512]{1,0:T(8,128)(2,1)S(1)}, bf16[384,512]{1,0:T(8,128)(2,1)}, u32[]{:S(2)}) copy-start(bf16[384,512]{1,0:T(8,128)(2,1)} %param.7) | copy-start | bytes 1179652
  6.5 145.1 %all-reduce.5.cloned.1.call-start = ((), (), s32[]{:S(2)}) async-start(), calls=%async_computation | async-start | bytes 6291456 | tf_op jit(solution)/shard_map/psum | solution.py:19
  13.1 3.2 copy-start
  19.8 9.1 %copy-start.5 = (f32[2,512]{1,0:T(2,128)S(1)}, f32[2,512]{1,0:T(2,128)}, u32[]{:S(2)}) copy-start(f32[2,512]{1,0:T(2,128)} %param.11) | copy-start | bytes 12292
  19.8 9.1 %copy-start.3 = (f32[2,4096]{1,0:T(2,128)S(1)}, f32[2,4096]{1,0:T(2,128)}, u32[]{:S(2)}) copy-start(f32[2,4096]{1,0:T(2,128)} %param.9) | copy-start | bytes 98308
  19.9 169.5 %all-reduce.7.cloned.1.call-start = ((), (), s32[]{:S(2)}) async-start(), calls=%async_computation.1 | async-start | bytes 786432 | tf_op jit(solution)/shard_map/psum | solution.py:24
  151.6 5.8 %copy-start.6 = (f32[2,512]{1,0:T(2,128)S(1)}, f32[2,512]{1,0:T(2,128)}, u32[]{:S(2)}) copy-start(f32[2,512]{1,0:T(2,128)} %param.13) | copy-start | bytes 12292
  157.4 185.6 %all-reduce.9.cloned.1.call-start = ((), (), s32[]{:S(2)}) async-start(), calls=%async_computation.2 | async-start | bytes 6291456 | tf_op jit(solution)/shard_map/psum | solution.py:19
  217.8 162.9 %all-reduce.11.cloned.1.call-start = ((), (), s32[]{:S(2)}) async-start(), calls=%async_computation.3 | async-start | bytes 786432 | tf_op jit(solution)/shard_map/psum | solution.py:24
  342.9 60.3 %copy-start.1 = (bf16[384,512]{1,0:T(8,128)(2,1)S(1)}, bf16[384,512]{1,0:T(8,128)(2,1)}, u32[]{:S(2)}) copy-start(bf16[384,512]{1,0:T(8,128)(2,1)} %all-reduce.7.cloned.1.call-done) | copy-start | bytes 1179652
Sparse Core Ops, SparseCore 0:
  19.9 131.6 all-reduce.4
  157.5 31.8 all-reduce.6
  217.9 124.9 all-reduce.8
  348.8 31.8 all-reduce.10
where the time goes:
time: 412 us
  waiting for transfers between devices  312 us (76%)
  blocking collectives  42.7 us (10%)
  matrix products  20.8 us (5%)
  other arithmetic  20 us (5%)
  between operations  13.2 us (3%)
    psum x2, waiting for transfers between devices, local(): lax.psum(partial_up.astype(jnp.bfloat16), 'ra').astype(jnp.float32)  248 us
    psum x2, waiting for transfers between devices, local(): lax.psum(partial_down.astype(jnp.bfloat16), 'cb').astype(jnp.float32)  63.9 us
    psum x2, blocking collectives, local(): post_squares = lax.psum(jnp.sum(branch_in * branch_in, axis=1), 'ra')  42.7 us
    another operation x2, other arithmetic  15.5 us
    dot_general x2, matrix products, local(): jnp.dot(hidden, down_matrix, preferred_element_type=jnp.float32)  11.4 us
    dot_general x2, matrix products, local(): partial_up = jnp.dot(scaled, up_matrix, preferred_element_type=jnp.float32)  9.37 us
  transfers between devices with their start and end apart: 4, of which 4 were waited for; matrix products, arithmetic and copies ran while one was open for 2% of the time, Pallas kernels for 0%

commit v1 on v0

--- a/solution.py
+++ b/solution.py
@@ -21,7 +21,9 @@
             jnp.bfloat16
         )
         partial_down = jnp.dot(hidden, down_matrix, preferred_element_type=jnp.float32)
-        summed = lax.psum(partial_down.astype(jnp.bfloat16), "cb").astype(jnp.float32)
+        summed = jnp.sum(lax.all_gather(partial_down.astype(jnp.bfloat16), "cb"), axis=0).astype(
+            jnp.float32
+        )
         branch_in = summed * down_scale[sublayer][None, :]
         post_squares = lax.psum(jnp.sum(branch_in * branch_in, axis=1), "ra")
         inv_post = lax.rsqrt(post_squares / model_width + norm_eps)[:, None]

time: 412 us -> 386 us (0.937)
  waiting for transfers between devices: 312 us -> 285 us
    psum x2 -> x0, waiting for transfers between devices: 63.9 us -> none  [local(): lax.psum(partial_down.astype(jnp.bfloat16), 'cb').astype(jnp.float32)]
    all_gather x0 -> x2, waiting for transfers between devices: none -> 37.6 us  [local(): lax.all_gather(partial_down.astype(jnp.bfloat16), 'cb')]
where the time goes in v1:
time: 386 us
  waiting for transfers between devices  285 us (74%)
  blocking collectives  42.7 us (11%)
  other arithmetic  20.7 us (5%)
  matrix products  20.6 us (5%)
  between operations  13.2 us (3%)
    psum x2, waiting for transfers between devices, local(): lax.psum(partial_up.astype(jnp.bfloat16), 'ra').astype(jnp.float32)  248 us
    psum x2, blocking collectives, local(): post_squares = lax.psum(jnp.sum(branch_in * branch_in, axis=1), 'ra')  42.7 us
    all_gather x2, waiting for transfers between devices, local(): lax.all_gather(partial_down.astype(jnp.bfloat16), 'cb')  37.6 us
    another operation x2, other arithmetic  15.5 us
    dot_general x2, matrix products, local(): jnp.dot(hidden, down_matrix, preferred_element_type=jnp.float32)  11.4 us
    dot_general x2, matrix products, local(): partial_up = jnp.dot(scaled, up_matrix, preferred_element_type=jnp.float32)  9.24 us
  transfers between devices with their start and end apart: 4, of which 4 were waited for; matrix products, arithmetic and copies ran while one was open for 2% of the time, Pallas kernels for 0%

profile of v1, /device:TPU:0, one launch (start us, length us, event | category | flops | bytes accessed | tf_op | source)
XLA Modules:
  0.0 385.9 jit_solution(16009735728048186631)
XLA Ops:
  6.5 6.5 %convert.10 = bf16[2,512,4096]{2,1,0:T(8,128)(2,1)S(1)} convert(f32[2,512,4096]{2,1,0:T(8,128)} %param.8) | non-fusion elementwise | flops 4194304 | bytes 25165824 | tf_op jit(solution)/shard_map/convert.5
  13.1 3.2 copy-done
  16.3 3.5 convolution_convert_fusion.1
  19.8 0.0 all-reduce.3.cloned.1.call-update
  19.8 0.0 all-gather.5.cloned.1.call-start
  19.9 9.0 %convert.11 = bf16[2,4096,512]{2,1,0:T(8,128)(2,1)} convert(f32[2,4096,512]{2,1,0:T(8,128)} %param.10) | non-fusion elementwise | flops 4194304 | bytes 25165824 | tf_op jit(solution)/shard_map/convert.4
  28.9 122.5 %all-reduce.3.cloned.1.call-done = bf16[384,4096]{1,0:T(8,128)(2,1)} async-done(((bf16[384,4096]{1,0:T(8,128)(2,1)}), bf16[384,4096]{1,0:T(8,128)(2,1)}) %all-reduce.3.cloned.1.call-update) | async-done | bytes 3145744 | tf_op jit(solution)/shard_map/psum | solution.py:19
  151.5 5.7 %fusion.6 = bf16[384,512]{1,0:T(8,128)(2,1)} fusion(bf16[2,4096,512]{2,1,0:T(8,128)(2,1)} %convert.11, bf16[384,4096]{1,0:T(8,128)(2,1)} %all-reduce.3.cloned.1.call-done, f32[4096]{0:T(1024)S(1)} %bitcast.34), kind=kOutput, calls=%fused_computation.14 | convolution fusion | flops 1618673664 | bytes 7749632 | tf_op jit(solution)/shard_map/dot_general | solution.py:23
  157.2 0.0 all-gather.5.cloned.1.call-update
  157.2 0.0 all-reduce.5.cloned.1.call-start
  157.3 18.7 %all-gather.5.cloned.1.call-done = bf16[1536,512]{1,0:T(8,128)(2,1)} async-done(((bf16[384,512]{1,0:T(8,128)(2,1)}), bf16[1536,512]{1,0:T(8,128)(2,1)}) %all-gather.5.cloned.1.call-update) | async-done | bytes 1572880 | tf_op jit(solution)/shard_map/all_gather | solution.py:24
  176.0 1.8 reduce_sum.42
  177.8 0.2 multiply_reduce_fusion.1
  178.0 21.3 %psum.29 = f32[384]{0:T(512)S(1)} all-reduce(f32[384]{0:T(512)S(1)} %multiply_reduce_fusion.1), channel_id=1, replica_groups=mesh['ra'=8,'cb'=4] {'ra'}, use_global_device_ids=true, to_apply=%region_3.4 | all-reduce | flops 384 | bytes 3072 | tf_op jit(solution)/shard_map/psum | solution.py:28
  199.4 5.7 %convolution_convert_fusion = bf16[384,4096]{1,0:T(8,128)(2,1)} fusion(bf16[2,512,4096]{2,1,0:T(8,128)(2,1)} %copy-done, f32[512]{0:T(512)S(1)} %bitcast.38, bf16[384,512]{1,0:T(8,128)(2,1)S(1)} %copy-done.1, bf16[384,512]{1,0:T(8,128)(2,1)S(1)} %reduce_sum.42, f32[512]{0:T(512)S(1)} %bitcast.36, f32[384]{0:T(512)S(1)} %add_rsqrt_fusion.1, f32[512]{0:T(512)S(1)} %bitcast.31), kind=kOutput, calls=%fused_computation.2 | convolution fusion | flops 1614348288 | bytes 8134144 | tf_op jit(solution)/shard_map/dot_general | solution.py:18
  205.1 0.0 all-reduce.5.cloned.1.call-update
  205.1 0.0 all-gather.7.cloned.1.call-start
  205.2 125.2 %all-reduce.5.cloned.1.call-done = bf16[384,4096]{1,0:T(8,128)(2,1)} async-done(((bf16[384,4096]{1,0:T(8,128)(2,1)}), bf16[384,4096]{1,0:T(8,128)(2,1)}) %all-reduce.5.cloned.1.call-update) | async-done | bytes 3145744 | tf_op jit(solution)/shard_map/psum | solution.py:19
  330.3 5.7 %fusion.7 = bf16[384,512]{1,0:T(8,128)(2,1)} fusion(bf16[2,4096,512]{2,1,0:T(8,128)(2,1)} %convert.11, bf16[384,4096]{1,0:T(8,128)(2,1)} %all-reduce.5.cloned.1.call-done, f32[4096]{0:T(1024)S(1)} %bitcast.33), kind=kOutput, calls=%fused_computation.15 | convolution fusion | flops 1618673664 | bytes 7749632 | tf_op jit(solution)/shard_map/dot_general | solution.py:23
  336.1 18.8 %all-gather.7.cloned.1.call-done = bf16[1536,512]{1,0:T(8,128)(2,1)} async-done(((bf16[384,512]{1,0:T(8,128)(2,1)}), bf16[1536,512]{1,0:T(8,128)(2,1)}) %all-gather.7.cloned.1.call-update) | async-done | bytes 1572880 | tf_op jit(solution)/shard_map/all_gather | solution.py:24
  354.9 1.8 reduce_sum.44
  356.7 0.2 multiply_reduce_fusion
  356.9 21.3 %psum.31 = f32[384]{0:T(512)S(1)} all-reduce(f32[384]{0:T(512)S(1)} %multiply_reduce_fusion), channel_id=1, replica_groups=mesh['ra'=8,'cb'=4] {'ra'}, use_global_device_ids=true, to_apply=%region_7.8 | all-reduce | flops 384 | bytes 3072 | tf_op jit(solution)/shard_map/psum | solution.py:28
  378.3 1.1 fusion.12
  (19 shorter events, 0.1 us)
Async XLA Ops:
  6.5 6.5 %copy-start.3 = (f32[2,512]{1,0:T(2,128)S(1)}, f32[2,512]{1,0:T(2,128)}, u32[]{:S(2)}) copy-start(f32[2,512]{1,0:T(2,128)} %param.12) | copy-start | bytes 12292
  6.5 9.8 %copy-start.1 = (bf16[384,512]{1,0:T(8,128)(2,1)S(1)}, bf16[384,512]{1,0:T(8,128)(2,1)}, u32[]{:S(2)}) copy-start(bf16[384,512]{1,0:T(8,128)(2,1)} %param.7) | copy-start | bytes 1179652
  6.5 144.9 %all-reduce.3.cloned.1.call-start = ((), (), s32[]{:S(2)}) async-start(), calls=%async_computation | async-start | bytes 6291456 | tf_op jit(solution)/shard_map/psum | solution.py:19
  13.1 3.2 copy-start
  19.8 9.1 %copy-start.2 = (f32[2,4096]{1,0:T(2,128)S(1)}, f32[2,4096]{1,0:T(2,128)}, u32[]{:S(2)}) copy-start(f32[2,4096]{1,0:T(2,128)} %param.9) | copy-start | bytes 98308
  19.8 156.2 %all-gather.5.cloned.1.call-start = ((), (), s32[]{:S(2)}) async-start(), calls=%async_computation.2 | async-start | bytes 1966080 | tf_op jit(solution)/shard_map/all_gather | solution.py:24
  151.4 5.8 %copy-start.4 = (f32[2,512]{1,0:T(2,128)S(1)}, f32[2,512]{1,0:T(2,128)}, u32[]{:S(2)}) copy-start(f32[2,512]{1,0:T(2,128)} %param.11) | copy-start | bytes 12292
  151.4 5.8 %copy-start.5 = (f32[2,512]{1,0:T(2,128)S(1)}, f32[2,512]{1,0:T(2,128)}, u32[]{:S(2)}) copy-start(f32[2,512]{1,0:T(2,128)} %param.13) | copy-start | bytes 12292
  157.2 173.2 %all-reduce.5.cloned.1.call-start = ((), (), s32[]{:S(2)}) async-start(), calls=%async_computation.1 | async-start | bytes 6291456 | tf_op jit(solution)/shard_map/psum | solution.py:19
  205.1 149.8 %all-gather.7.cloned.1.call-start = ((), (), s32[]{:S(2)}) async-start(), calls=%async_computation.3 | async-start | bytes 1966080 | tf_op jit(solution)/shard_map/all_gather | solution.py:24
Sparse Core Ops, SparseCore 0:
  19.9 131.4 all-reduce.2
  157.3 18.6 all-gather.4
  205.3 125.0 all-reduce.4
  336.2 18.6 all-gather.6
